TPU v7x, 256 devices: a whole 4x4x8 slice. The times are simulated.
256 devices in a mesh: sp: 64 (over z, y, core), tp: 4 (over x).
Axes of the slice: x: 4, y: 4, z: 8, core: 2. Of those that a mesh axis runs over, the one named last changes fastest.
Arguments:
- tokens: bfloat16 [10240, 2048], P('sp'), may hold values from -6 to 6
- input_gain: float32 [2048], replicated, may hold values from 0.1 to 1.9
- chain_query: bfloat16 [2048, 1024], P('sp', 'tp'), may hold values from -0.125 to 0.125
- forward_gate: bfloat16 [2048, 1024], P('sp', 'tp'), may hold values from -0.125 to 0.125
- backward_gate: bfloat16 [2048, 1024], P('sp', 'tp'), may hold values from -0.125 to 0.125
- chain_value: bfloat16 [2048, 1024], P('sp', 'tp'), may hold values from -0.125 to 0.125
- output_gate: bfloat16 [2048, 1024], P('sp', 'tp'), may hold values from -0.125 to 0.125
- forget_rate: float32 [2, 1024], P(None, 'tp'), may hold values from 0.2 to 6
- chain_gain: float32 [1024], P('tp'), may hold values from 0.1 to 1.9
- query_down: bfloat16 [2048, 768], P('sp'), may hold values from -0.125 to 0.125
- latent_down: bfloat16 [2048, 512], P('sp'), may hold values from -0.125 to 0.125
- rotary_down: bfloat16 [2048, 64], replicated, may hold values from -0.125 to 0.125
- query_latent_gain: float32 [768], replicated, may hold values from 0.1 to 1.9
- latent_gain: float32 [512], replicated, may hold values from 0.1 to 1.9
- query_up: bfloat16 [768, 1536], P(None, 'tp'), may hold values from -0.21875 to 0.21875
- latent_up: bfloat16 [512, 2048], P(None, 'tp'), may hold values from -0.25 to 0.25
- query_head_gain: float32 [192], replicated, may hold values from 0.1 to 1.9
- key_head_gain: float32 [192], replicated, may hold values from 0.1 to 1.9
- mixer_gain: float32 [1024], P('tp'), may hold values from 0.1 to 1.9
- chain_out: bfloat16 [1024, 2048], P('tp', 'sp'), may hold values from -0.125 to 0.125
- attend_out: bfloat16 [1024, 2048], P('tp', 'sp'), may hold values from -0.125 to 0.125
Outputs:
- mixed: float32 [10240, 2048], P(('sp', 'tp'))
All inputs are finite; a program needn't handle non-finite values.
Results may differ from a plain program's by a relative error of at most 0.017.
Values may be sent and summed in bfloat16 or wider, within the bound.
No kernel may reach another device: no remote copies, remote signals or barrier semaphores. Data moves between devices by JAX's collectives and lax.ppermute only.
A program may use at most 128 MiB of HBM per device.

v0:
```python
import jax
import jax.numpy as jnp
from jax import lax
from jax.sharding import Mesh
from jax.sharding import PartitionSpec as P

KEY_DIM = 128
VAL_DIM = 128
NOPE_DIM = 128
ROPE_DIM = 64
VHEAD_DIM = 128
ATT_QK = 192
SP = ("sp_0", "sp_1", "sp_2")
SP_TP = ("sp_0", "sp_1", "sp_2", "tp")
norm_eps = 1e-06
rope_theta = 10000.0
finest_arithmetic_mode = lax.Precision.HIGHEST


def turned_gather(arrays, axis, dims):
    turned = [jnp.moveaxis(a, dim, 0) for a, dim in zip(arrays, dims)]
    both = jnp.concatenate([t.reshape(len(t), -1) for t in turned], axis=1)
    filled, at, done = (lax.all_gather(both, axis, axis=0, tiled=True), 0, [])
    for t, dim in zip(turned, dims):
        share = filled[:, at : at + t[0].size].reshape(-1, *t.shape[1:])
        done.append(jnp.moveaxis(share, 0, dim))
        at += t[0].size
    return tuple(done)


def filled_with(value, identity):
    return jax.tree.map(
        lambda part, zero: jnp.zeros_like(part) + jnp.asarray(zero, part.dtype), value, identity
    )


def carried_in(value, axes, combine, identity, reverse):
    before = start = filled_with(value, identity)
    total = value
    for axis in reversed(axes):
        count, position = (lax.axis_size(axis), lax.axis_index(axis))
        pieces = jax.tree.map(lambda part: lax.all_gather(part, axis), total)
        inside, total = (start, start)
        for k in reversed(range(count)) if reverse else range(count):
            passed = k > position if reverse else k < position
            total = combine(total, jax.tree.map(lambda part: part[k], pieces))
            inside = jax.tree.map(lambda new, old: jnp.where(passed, new, old), total, inside)
        before = combine(inside, before)
    return before


def side_by_side(arrays, axis, dim, along):
    ends, at = ([], 0)
    for a in arrays[:-1]:
        at += a.shape[along]
        ends.append(at)
    both = jnp.concatenate(arrays, axis=along)
    return tuple(jnp.split(lax.all_gather(both, axis, axis=dim, tiled=True), ends, axis=along))


def in_blocks(value, dim, count):
    before, after = (value.shape[:dim], value.shape[dim + 1 :])
    return jnp.moveaxis(value.reshape(*before, count, -1, *after), dim, 0)


def sent_and_summed(value, axis, dim):
    count = lax.axis_size(axis)
    pieces = lax.all_to_all(in_blocks(value, dim, count), axis, 0, 0, tiled=True)
    return jnp.sum(pieces, axis=0)


def rms_scale(values, gain_vec):
    mean_square = jnp.mean(values * values, axis=-1, keepdims=True)
    return values * lax.rsqrt(mean_square + norm_eps) * gain_vec


def rotate_tail(values, positions):
    half_dim = ROPE_DIM // 2
    inverse = rope_theta ** (-jnp.arange(0, ROPE_DIM, 2).astype(jnp.float32) / ROPE_DIM)
    angles = positions.astype(jnp.float32)[:, None] * inverse
    cosine = jnp.cos(angles)[:, None, :]
    sine_table = jnp.sin(angles)[:, None, :]
    unrotated = values[..., :NOPE_DIM]
    first_half = values[..., NOPE_DIM : NOPE_DIM + half_dim]
    latter_element = values[..., NOPE_DIM + half_dim :]
    return jnp.concatenate(
        [
            unrotated,
            first_half * cosine - latter_element * sine_table,
            latter_element * cosine + first_half * sine_table,
        ],
        axis=-1,
    )


def gate_parts(pre_gate, rate_row, seq_len):
    opening = rate_row / seq_len * jax.nn.sigmoid(-pre_gate.astype(jnp.float32))
    return (jnp.log1p(-opening), opening)


def summarize(query_rows, key_rows, payload_array_lines, log_decay):
    cumulative = jnp.cumsum(log_decay, axis=0)
    weighted_probe_vectors = query_rows * jnp.exp(cumulative)
    weighted_lookup_vectors = key_rows * jnp.exp(-cumulative)
    overall_shrink_multiplier = jnp.exp(cumulative[-1])
    recurrent_memory_digest = overall_shrink_multiplier[:, :, None] * jnp.einsum(
        "jre,jrw->rew",
        weighted_lookup_vectors,
        payload_array_lines,
        precision=finest_arithmetic_mode,
    )
    return (
        weighted_probe_vectors,
        weighted_lookup_vectors,
        overall_shrink_multiplier,
        recurrent_memory_digest,
    )


def emit(weighted_probe_vectors, weighted_lookup_vectors, payload_array_lines, incoming_update):
    length = weighted_probe_vectors.shape[0]
    lower_mask = jnp.tril(jnp.ones((length, length), jnp.float32))
    scores = (
        jnp.einsum(
            "thk,shk->hts",
            weighted_probe_vectors,
            weighted_lookup_vectors,
            precision=finest_arithmetic_mode,
        )
        * lower_mask
    )
    within = jnp.einsum(
        "hts,shv->thv", scores, payload_array_lines, precision=finest_arithmetic_mode
    )
    prior_state = jnp.einsum(
        "mjf,jfi->mji", weighted_probe_vectors, incoming_update, precision=finest_arithmetic_mode
    )
    return within + prior_state


def chain_combine(earlier, following):
    return (earlier[0] * following[0], following[0][:, :, None] * earlier[1] + following[1])


def add_scores(running, query_final, key_piece, value_piece):
    score_scale = query_final.shape[-1] ** (-0.5)
    scores = (
        jnp.einsum("qhd,khd->hqk", query_final, key_piece, preferred_element_type=jnp.float32)
        * score_scale
    )
    weights = jnp.exp(scores)
    numerator = running[0] + jnp.einsum(
        "hqk,khv->qhv",
        weights.astype(jnp.bfloat16),
        value_piece,
        preferred_element_type=jnp.float32,
    )
    return (numerator, running[1] + jnp.sum(weights, axis=-1))


def on_device(
    tokens,
    input_gain,
    chain_query,
    forward_gate,
    backward_gate,
    chain_value,
    output_gate,
    forget_rate,
    chain_gain,
    query_down,
    latent_down,
    rotary_down,
    query_latent_gain,
    latent_gain,
    query_up,
    latent_up,
    query_head_gain,
    key_head_gain,
    mixer_gain,
    chain_out,
    attend_out,
):
    gathered = turned_gather(
        (
            chain_query,
            forward_gate,
            backward_gate,
            chain_value,
            output_gate,
            query_down,
            latent_down,
            chain_out,
            attend_out,
        ),
        SP,
        (0, 0, 0, 0, 0, 0, 0, 1, 1),
    )
    (
        full_query,
        full_forward,
        full_backward,
        full_value,
        full_outgate,
        full_query_down,
        full_latent_down,
        full_chain_out,
        full_attend_out,
    ) = gathered
    tok_rows = tokens.shape[0]
    seq_len = tok_rows * lax.axis_size(SP)
    normed = rms_scale(tokens.astype(jnp.float32), input_gain).astype(jnp.bfloat16)

    def project(source, weight):
        return jnp.dot(source, weight, preferred_element_type=jnp.float32).astype(jnp.bfloat16)

    def heads_of(tensor, head_width):
        return tensor.astype(jnp.float32).reshape(
            tok_rows, tensor.shape[1] // head_width, head_width
        )

    def row_term(source, weight):
        return jnp.dot(source, weight, preferred_element_type=jnp.float32)

    query_rows = heads_of(project(normed, full_query), KEY_DIM)
    payload_array_lines = heads_of(project(normed, full_value), VAL_DIM)
    forward_log, forward_key = gate_parts(project(normed, full_forward), forget_rate[0], seq_len)
    backward_log, backward_key = gate_parts(project(normed, full_backward), forget_rate[1], seq_len)
    gate_logit = project(normed, full_outgate).astype(jnp.float32)
    chain_heads = query_rows.shape[1]
    identity = (
        jnp.ones((chain_heads, KEY_DIM), jnp.float32),
        jnp.zeros((chain_heads, KEY_DIM, VAL_DIM), jnp.float32),
    )
    forward_parts = summarize(
        query_rows,
        heads_of(forward_key, KEY_DIM),
        payload_array_lines,
        heads_of(forward_log, KEY_DIM),
    )
    forward_in = carried_in(
        (forward_parts[2], forward_parts[3]), SP, chain_combine, identity, False
    )[1]
    flipped_values = jnp.flip(payload_array_lines, 0)
    backward_parts = summarize(
        jnp.flip(query_rows, 0),
        jnp.flip(heads_of(backward_key, KEY_DIM), 0),
        flipped_values,
        jnp.flip(heads_of(backward_log, KEY_DIM), 0),
    )
    backward_in = carried_in(
        (backward_parts[2], backward_parts[3]), SP, chain_combine, identity, True
    )[1]
    combined = emit(forward_parts[0], forward_parts[1], payload_array_lines, forward_in) + jnp.flip(
        emit(backward_parts[0], backward_parts[1], flipped_values, backward_in), 0
    )
    head_gain = chain_gain.reshape(chain_heads, VAL_DIM)
    chain_mixed = (
        rms_scale(combined, head_gain).reshape(tok_rows, -1) * jax.nn.silu(gate_logit)
    ).astype(jnp.bfloat16)
    raw_query_latent = project(normed, full_query_down)
    raw_pair_latent = project(normed, full_latent_down)
    query_latent = rms_scale(raw_query_latent.astype(jnp.float32), query_latent_gain).astype(
        jnp.bfloat16
    )
    pair_latent = rms_scale(raw_pair_latent.astype(jnp.float32), latent_gain).astype(jnp.bfloat16)
    rotary_key = project(normed, rotary_down).astype(jnp.float32)
    attend_heads = query_up.shape[1] // ATT_QK
    attend_query = (
        project(query_latent, query_up).astype(jnp.float32).reshape(tok_rows, attend_heads, ATT_QK)
    )
    attend_pairs = project(pair_latent, latent_up).reshape(
        tok_rows, attend_heads, NOPE_DIM + VHEAD_DIM
    )
    positions = lax.axis_index(SP) * tok_rows + jnp.arange(tok_rows, dtype=jnp.int32)
    query_final = rotate_tail(rms_scale(attend_query, query_head_gain), positions).astype(
        jnp.bfloat16
    )
    key_cat = jnp.concatenate(
        [
            attend_pairs[..., :NOPE_DIM].astype(jnp.float32),
            jnp.broadcast_to(rotary_key[:, None, :], (tok_rows, attend_heads, ROPE_DIM)),
        ],
        axis=-1,
    )
    key_final = rotate_tail(rms_scale(key_cat, key_head_gain), positions).astype(jnp.bfloat16)
    keys_flat = key_final.reshape(tok_rows, attend_heads * ATT_QK)
    values_flat = attend_pairs[..., NOPE_DIM:].reshape(tok_rows, attend_heads * VHEAD_DIM)
    start_sum = (
        jnp.zeros((tok_rows, attend_heads, VHEAD_DIM), jnp.float32),
        jnp.zeros((attend_heads, tok_rows), jnp.float32),
    )
    pieces = side_by_side((keys_flat, values_flat), SP, 0, 1)
    key_piece = pieces[0].reshape(pieces[0].shape[0], attend_heads, ATT_QK)
    value_piece = pieces[1].reshape(pieces[1].shape[0], attend_heads, VHEAD_DIM)
    piece_rows = key_piece.shape[0]
    span_rows = 1024

    def one_span(partial_sum, interval_couple):
        return (add_scores(partial_sum, query_final, interval_couple[0], interval_couple[1]), None)

    shaped = (
        key_piece.reshape(piece_rows // span_rows, span_rows, attend_heads, ATT_QK),
        value_piece.reshape(piece_rows // span_rows, span_rows, attend_heads, VHEAD_DIM),
    )
    result, _ = lax.scan(one_span, start_sum, shaped)
    numerator, denominator = result
    attend_rows = numerator / jnp.transpose(denominator)[:, :, None]
    attend_mixed = (
        rms_scale(attend_rows, mixer_gain.reshape(attend_heads, VHEAD_DIM))
        .reshape(tok_rows, attend_heads * VHEAD_DIM)
        .astype(jnp.bfloat16)
    )
    return sent_and_summed(
        row_term(chain_mixed, full_chain_out) + row_term(attend_mixed, full_attend_out), "tp", 0
    )


def solution(mesh):
    torus = Mesh(mesh.devices.reshape(8, 4, 2, mesh.shape["tp"]), ("sp_0", "sp_1", "sp_2", "tp"))
    placed = (
        P(SP, None),
        P(),
        P(SP, "tp"),
        P(SP, "tp"),
        P(SP, "tp"),
        P(SP, "tp"),
        P(SP, "tp"),
        P(None, "tp"),
        P("tp"),
        P(SP, None),
        P(SP, None),
        P(),
        P(),
        P(),
        P(None, "tp"),
        P(None, "tp"),
        P(),
        P(),
        P("tp"),
        P("tp", SP),
        P("tp", SP),
    )
    return jax.shard_map(
        on_device, mesh=torus, in_specs=placed, out_specs=P(SP_TP, None), check_vma=False
    )
```

profile of v0, /device:TPU:1, one launch (start us, length us, event | category | flops | bytes accessed | tf_op | source)
XLA Modules:
  0.0 444.4 jit_solution(1386294659774863667)
XLA Ops:
  6.5 0.8 constant_dynamic-update-slice_fusion.8
  10.2 0.8 constant_dynamic-update-slice_fusion.3
  11.0 0.8 constant_dynamic-update-slice_fusion.2
  11.8 0.7 constant_dynamic-update-slice_fusion.1
  14.0 1.3 fusion.11
  15.3 1.6 fusion.44
  16.9 0.7 copy.104
  17.6 1.0 multiply_cosine_fusion
  18.7 89.1 %all-gather.7.cloned.1.call-done = bf16[2048,3072]{1,0:T(8,128)(2,1)} async-done(((bf16[32,3072]{1,0:T(8,128)(2,1)}), bf16[2048,3072]{1,0:T(8,128)(2,1)}) %all-gather.7.cloned.1.call-update) | async-done | bytes 12582928 | tf_op jit(solution)/shard_map/all_gather | solution.py:23
  107.8 1.6 fusion.35
  110.6 1.8 all_gather.66
  112.4 5.8 %all_gather.67 = f32[4,2,128]{2,1,0:T(2,128)S(1)} all-gather(f32[1,2,128]{2,1,0:T(2,128)S(1)} %get-tuple-element.137), channel_id=1, replica_groups=mesh['sp_0'=8,'sp_1'=4,'sp_2'=2,'tp'=4] {'sp_1'}, dimensions={0}, use_global_device_ids=true | all-gather | bytes 5120 | tf_op jit(solution)/shard_map/all_gather | solution.py:42
  118.2 1.6 fusion.40
  120.3 3.7 all_gather.59
  124.1 1.6 fusion.43
  126.7 2.0 all-gather.1
  128.7 2.4 multiply_reduce_fusion.2
  132.1 9.9 %all_gather.71 = f32[4,2,128,128]{3,2,1,0:T(8,128)S(1)} all-gather(f32[1,2,128,128]{3,2,1,0:T(8,128)S(1)} %bitcast_add_fusion.4), channel_id=1, replica_groups=mesh['sp_0'=8,'sp_1'=4,'sp_2'=2,'tp'=4] {'sp_1'}, dimensions={0}, use_global_device_ids=true | all-gather | bytes 655360 | tf_op jit(solution)/shard_map/all_gather | solution.py:42
  142.0 0.9 multiply_add_fusion
  142.9 6.5 %all_gather.60 = f32[4,2,128]{2,1,0:T(2,128)S(1)} all-gather(f32[1,2,128]{2,1,0:T(2,128)S(1)} %get-tuple-element.132), channel_id=1, replica_groups=mesh['sp_0'=8,'sp_1'=4,'sp_2'=2,'tp'=4] {'sp_1'}, dimensions={0}, use_global_device_ids=true | all-gather | bytes 5120 | tf_op jit(solution)/shard_map/all_gather | solution.py:42
  149.9 6.5 %all-gather = f32[4,128,128]{2,1,0:T(8,128)S(1)} all-gather(f32[2,128,128]{2,1,0:T(8,128)S(1)} %convolution_multiply_fusion.4), channel_id=2, replica_groups=mesh['sp_0'=8,'sp_1'=4,'sp_2'=2,'tp'=4] {'sp_2'}, dimensions={0}, use_global_device_ids=true | all-gather | bytes 393216 | tf_op jit(solution)/shard_map/all_gather | solution.py:42
  157.1 10.3 %all_gather.64 = f32[4,2,128,128]{3,2,1,0:T(8,128)S(1)} all-gather(f32[1,2,128,128]{3,2,1,0:T(8,128)S(1)} %bitcast_add_fusion.10), channel_id=1, replica_groups=mesh['sp_0'=8,'sp_1'=4,'sp_2'=2,'tp'=4] {'sp_1'}, dimensions={0}, use_global_device_ids=true | all-gather | bytes 655360 | tf_op jit(solution)/shard_map/all_gather | solution.py:42
  167.5 0.9 multiply_add_fusion.1
  168.5 3.1 multiply_reduce_fusion
  173.8 0.8 subtract_convert_fusion
  176.5 1.9 fusion.42
  178.4 1.4 rev.17
  179.7 11.8 %all_gather.68 = f32[8,2,128]{2,1,0:T(2,128)S(1)} all-gather(f32[1,2,128]{2,1,0:T(2,128)S(1)} %get-tuple-element.126), channel_id=1, replica_groups=mesh['sp_0'=8,'sp_1'=4,'sp_2'=2,'tp'=4] {'sp_0'}, dimensions={0}, use_global_device_ids=true | all-gather | bytes 9216 | tf_op jit(solution)/shard_map/all_gather | solution.py:42
  191.5 10.5 %all_gather.61 = f32[8,2,128]{2,1,0:T(2,128)S(1)} all-gather(f32[1,2,128]{2,1,0:T(2,128)S(1)} %get-tuple-element.121), channel_id=1, replica_groups=mesh['sp_0'=8,'sp_1'=4,'sp_2'=2,'tp'=4] {'sp_0'}, dimensions={0}, use_global_device_ids=true | all-gather | bytes 9216 | tf_op jit(solution)/shard_map/all_gather | solution.py:42
  202.0 0.8 pad_maximum_fusion.3
  203.8 2.4 fusion.76
  206.9 8.0 %all-gather.9.cloned.1.call-done = f32[8,2,128,128]{3,2,1,0:T(8,128)} async-done(((f32[1,2,128,128]{3,2,1,0:T(8,128)}), f32[8,2,128,128]{3,2,1,0:T(8,128)}) %all-gather.9.cloned.1.call-update) | async-done | bytes 1048592 | tf_op jit(solution)/shard_map/all_gather | solution.py:42
  214.9 2.3 fusion.89
  217.7 2.8 fusion.46
  220.4 91.5 %all-gather.13.cloned.1.call-done = bf16[10240,640]{1,0:T(8,128)(2,1)} async-done(((bf16[160,640]{1,0:T(8,128)(2,1)}), bf16[10240,640]{1,0:T(8,128)(2,1)}) %all-gather.13.cloned.1.call-update) | async-done | bytes 13107216 | tf_op jit(solution)/shard_map/all_gather | solution.py:58
  312.0 4.3 split.8
  316.2 8.3 %reshape_reshape.6 = bf16[10,1024,2,128]{3,2,1,0:T(2,128)(2,1)} reshape(bf16[10240,256]{1,0:T(8,128)(2,1)} %split.8) | data formatting | bytes 10485760 | tf_op jit(solution)/shard_map/reshape;reshape | solution.py:304
  324.6 6.9 %split.9 = bf16[10240,384]{1,0:T(8,128)(2,1)} slice(bf16[10240,640]{1,0:T(8,128)(2,1)} %all-gather.13.cloned.1.call-done), slice={[0:10240], [0:384]} | slice | bytes 15728640 | tf_op jit(solution)/shard_map/split | solution.py:58
  331.4 22.6 %reshape_reshape.7 = bf16[10,1024,2,192]{3,2,1,0:T(2,128)(2,1)} reshape(bf16[10240,384]{1,0:T(8,128)(2,1)} %split.9) | data formatting | bytes 15728640 | tf_op jit(solution)/shard_map/reshape;reshape | solution.py:303
  354.1 25.7 %copy.109 = bf16[10,1024,2,192]{1,3,2,0:T(8,128)(2,1)} copy(bf16[10,1024,2,192]{3,2,1,0:T(2,128)(2,1)} %reshape_reshape.7) | data formatting | bytes 15728640
  379.7 34.0 %while.13 = (s32[]{:T(128)}, f32[160,2,128]{2,0,1:T(8,128)S(1)}, f32[2,160]{1,0:T(2,128)S(1)}, bf16[10,1024,2,128]{3,2,1,0:T(2,128)(2,1)}, bf16[10,1024,2,192]{1...) while((s32[]{:T(128)}, f32[160,2,128]{2,0,1:T(8,128)S(1)}, ...), condition=%wide.region_12.13_spmd.clone, body=%wide.region_10.12_spmd.clone.sunk | while | flops 210780480 | bytes 4125808 | solution.py:306
  379.7 1.4 constant_dynamic-slice_fusion.2
  381.2 1.6 fusion.302
  383.1 1.4 constant_dynamic-slice_fusion.2
  384.6 1.6 fusion.302
  386.5 1.4 constant_dynamic-slice_fusion.2
  387.9 1.6 fusion.302
  389.9 1.4 constant_dynamic-slice_fusion.2
  391.3 1.6 fusion.302
  393.3 1.4 constant_dynamic-slice_fusion.2
  394.7 1.6 fusion.302
  396.7 1.4 constant_dynamic-slice_fusion.2
  398.1 1.6 fusion.302
  400.1 1.4 constant_dynamic-slice_fusion.2
  401.5 1.6 fusion.302
  403.5 1.4 constant_dynamic-slice_fusion.2
  404.9 1.6 fusion.302
  406.9 1.4 constant_dynamic-slice_fusion.2
  408.3 1.6 fusion.302
  410.3 1.4 constant_dynamic-slice_fusion.2
  411.7 1.6 fusion.302
  414.0 1.7 convolution_add_fusion
  415.7 21.4 %all_to_all.5 = f32[4,40,2048]{2,1,0:T(8,128)S(1)} all-to-all(f32[4,40,2048]{2,1,0:T(8,128)S(1)} %bitcast.436), channel_id=1, replica_groups=mesh['sp_0'=8,'sp_1'=4,'sp_2'=2,'tp'=4] {'tp'}, dimensions={0} | all-to-all | bytes 2621440 | tf_op jit(solution)/shard_map/all_to_all | solution.py:68
  437.1 0.8 reduce_sum.88
  (175 shorter events, 19.2 us)
Async XLA Ops:
  6.5 165.7 %copy-start = (bf16[768,384]{1,0:T(8,128)(2,1)S(1)}, bf16[768,384]{1,0:T(8,128)(2,1)}, u32[]{:S(2)}) copy-start(bf16[768,384]{1,0:T(8,128)(2,1)} %param.37) | copy-start | bytes 1769476
  6.5 101.2 %all-gather.7.cloned.1.call-start = ((), (), s32[]{:S(2)}) async-start(), calls=%async_computation.1 | async-start | bytes 12779520 | tf_op jit(solution)/shard_map/all_gather | solution.py:23
  11.0 6.6 %copy-start.19 = (f32[2,256]{1,0:T(2,128)S(1)}, f32[2,256]{1,0:T(2,128)}, u32[]{:S(2)}) copy-start(f32[2,256]{1,0:T(2,128)} %param.30) | copy-start | bytes 6148
  13.2 0.7 copy-start.15
  13.2 94.6 %copy-start.6 = (bf16[160,2048]{1,0:T(8,128)(2,1)S(1)}, bf16[160,2048]{1,0:T(8,128)(2,1)}, u32[]{:S(2)}) copy-start(bf16[160,2048]{1,0:T(8,128)(2,1)} %param.23) | copy-start | bytes 1966084
  13.2 94.6 %copy-start.29 = (f32[2048]{0:T(1024)S(1)}, f32[2048]{0:T(1024)}, u32[]{:S(2)}) copy-start(f32[2048]{0:T(1024)} %param.24) | copy-start | bytes 24580
  13.9 189.8 %all-gather.11.cloned.1.call-start = ((), (), s32[]{:S(2)}) async-start(), calls=%async_computation.3 | async-start | bytes 1179648 | tf_op jit(solution)/shard_map/all_gather | solution.py:42
  15.3 153.2 %copy-start.23 = (f32[160]{0:T(256)}, f32[160]{0:T(256)S(1)}, u32[]{:S(2)}) copy-start(f32[160]{0:T(256)S(1)} %add_rsqrt_fusion.6) | copy-start | bytes 1924
  128.7 3.3 copy-start.2
  128.7 2.4 copy-start.7
  128.7 2.4 copy-start.18
  142.9 72.0 %all-gather.9.cloned.1.call-start = ((), (), s32[]{:S(2)}) async-start(), calls=%async_computation.2 | async-start | bytes 1179648 | tf_op jit(solution)/shard_map/all_gather | solution.py:42
  149.9 18.6 %copy-start.30 = (f32[2048]{0:T(1024)S(1)}, f32[2048]{0:T(1024)}, u32[]{:S(2)}) copy-start(f32[2048]{0:T(1024)} %param.24) | copy-start | bytes 24580
  168.4 3.8 copy-start.17
  168.4 143.6 %all-gather.13.cloned.1.call-start = ((), (), s32[]{:S(2)}) async-start(), calls=%async_computation.4 | async-start | bytes 13312000 | tf_op jit(solution)/shard_map/all_gather | solution.py:58
  172.2 1.0 copy-start.12
  172.2 1.2 copy-start.20
  172.6 0.9 copy-start.21
  172.8 0.9 copy-start.8
  172.8 0.9 copy-start.9
  173.6 1.4 copy-start.13
  173.8 2.7 copy-start.24
  173.8 2.7 copy-start.31
  176.4 25.5 %copy-start.10 = (bf16[160,2,32]{2,0,1:T(8,128)(2,1)S(1)}, bf16[160,2,32]{2,0,1:T(8,128)(2,1)}, u32[]{:S(2)}) copy-start(bf16[160,2,32]{2,0,1:T(8,128)(2,1)} %get-tuple-element.97) | copy-start | bytes 61444
  176.4 25.5 %copy-start.11 = (bf16[160,2,32]{2,0,1:T(8,128)(2,1)S(1)}, bf16[160,2,32]{2,0,1:T(8,128)(2,1)}, u32[]{:S(2)}) copy-start(bf16[160,2,32]{2,0,1:T(8,128)(2,1)} %get-tuple-element.98) | copy-start | bytes 61444
  176.4 25.5 %copy-start.14 = (bf16[160,2,128]{2,0,1:T(8,128)(2,1)S(1)}, bf16[160,2,128]{2,0,1:T(8,128)(2,1)}, u32[]{:S(2)}) copy-start(bf16[160,2,128]{2,0,1:T(8,128)(2,1)} %slice.707) | copy-start | bytes 245764
  178.3 24.4 %copy-start.3 = (f32[20,2,8,128]{3,2,1,0:T(8,128)}, f32[20,2,8,128]{3,2,1,0:T(8,128)S(1)}, u32[]{:S(2)}) copy-start(f32[20,2,8,128]{3,2,1,0:T(8,128)S(1)} %fusion.42) | copy-start | bytes 491524
  179.7 23.5 %copy-start.5 = (f32[160,2,128]{2,0,1:T(8,128)S(1)}, f32[160,2,128]{2,0,1:T(8,128)}, u32[]{:S(2)}) copy-start(f32[160,2,128]{2,0,1:T(8,128)} %rev.17) | copy-start | bytes 491524
  202.0 1.7 copy-start.27
  202.0 1.7 copy-start.28
  203.7 11.1 %copy-start.4 = (f32[20,2,8,128]{3,2,1,0:T(8,128)S(1)}, f32[20,2,8,128]{3,2,1,0:T(8,128)}, u32[]{:S(2)}) copy-start(f32[20,2,8,128]{3,2,1,0:T(8,128)} %copy-done.3) | copy-start | bytes 491524
  203.8 11.1 %copy-start.25 = (f32[2,128]{1,0:T(2,128)S(1)}, f32[2,128]{1,0:T(2,128)}, u32[]{:S(2)}) copy-start(f32[2,128]{1,0:T(2,128)} %get-tuple-element.91) | copy-start | bytes 3076
  203.8 11.1 %copy-start.26 = (f32[2,128]{1,0:T(2,128)S(1)}, f32[2,128]{1,0:T(2,128)}, u32[]{:S(2)}) copy-start(f32[2,128]{1,0:T(2,128)} %get-tuple-element.92) | copy-start | bytes 3076
  214.9 2.8 copy-start.32
  214.9 2.8 copy-start.33
  354.1 25.7 %copy-start.16 = (bf16[160,2,192]{2,0,1:T(8,128)(2,1)S(1)}, bf16[160,2,192]{2,0,1:T(8,128)(2,1)}, u32[]{:S(2)}) copy-start(bf16[160,2,192]{2,0,1:T(8,128)(2,1)} %pad_maximum_fusion.3) | copy-start | bytes 368644
  379.7 34.3 %copy-start.22 = (f32[256]{0:T(256)S(1)}, f32[256]{0:T(256)}, u32[]{:S(2)}) copy-start(f32[256]{0:T(256)} %param.41) | copy-start | bytes 3076
  415.7 22.2 %copy-start.1 = (bf16[768,384]{1,0:T(8,128)(2,1)S(1)}, bf16[768,384]{1,0:T(8,128)(2,1)}, u32[]{:S(2)}) copy-start(bf16[768,384]{1,0:T(8,128)(2,1)} %param.37) | copy-start | bytes 1769476
Sparse Core Ops, SparseCore 0:
  14.0 93.7 all-gather.6
  143.0 33.1 all-gather.10
  178.0 36.7 all-gather.8
  217.5 94.4 all-gather.12
where the time goes:
time: 448 us; the launch traced here: 444 us
  waiting for transfers between devices  189 us (42%)
  local copies, waits for them, and re-layouts  95 us (21%)
  blocking collectives  90.2 us (20%)
  matrix products  45.8 us (10%)
  between operations  13.9 us (3%)
  other arithmetic  10.4 us (2%)
    all_gather x1, waiting for transfers between devices, side_by_side(): lax.all_gather(both, axis, axis=dim, tiled=True)  91.5 us
    all_gather x1, waiting for transfers between devices, turned_gather(): filled, at, done = (lax.all_gather(both, axis, axis=0, tiled=True), 0, [])  89.1 us
    all_gather x10, blocking collectives, carried_in(): pieces = jax.tree.map(lambda part: lax.all_gather(part, axis), total)  68.8 us
    unnamed x78, local copies, waits for them, and re-layouts  33.2 us
    another operation x1, local copies, waits for them, and re-layouts, on_device(): key_piece.reshape(piece_rows // span_rows, span_rows, attend_heads, ATT_QK)  22.6 us
    all_to_all x1, blocking collectives, sent_and_summed(): lax.all_to_all(in_blocks(value, dim, count), axis, 0, 0, tiled=True)  21.4 us
    dot_general x10, matrix products, add_scores(): jnp.einsum('qhd,khd->hqk', query_final, key_piece, preferred_element_type...  16 us
    dot_general x9, matrix products, project(): jnp.dot(source, weight, preferred_element_type=jnp.float32)  14.4 us
  transfers between devices with their start and end apart: 4, of which 3 were waited for; matrix products, arithmetic and copies ran while one was open for 6% of the time, Pallas kernels for 0%

commit v1 on v0

--- a/solution.py
+++ b/solution.py
@@ -17,10 +17,17 @@
 finest_arithmetic_mode = lax.Precision.HIGHEST
 
 
+def exchange_gather(x, axis, dim):
+    size = lax.axis_size(axis)
+    parts = jnp.stack([x for _ in range(size)])
+    parts = lax.all_to_all(parts, axis, split_axis=0, concat_axis=0)
+    return jnp.concatenate(parts, axis=dim)
+
+
 def turned_gather(arrays, axis, dims):
     turned = [jnp.moveaxis(a, dim, 0) for a, dim in zip(arrays, dims)]
     both = jnp.concatenate([t.reshape(len(t), -1) for t in turned], axis=1)
-    filled, at, done = (lax.all_gather(both, axis, axis=0, tiled=True), 0, [])
+    filled, at, done = (exchange_gather(both, axis, 0), 0, [])
     for t, dim in zip(turned, dims):
         share = filled[:, at : at + t[0].size].reshape(-1, *t.shape[1:])
         done.append(jnp.moveaxis(share, 0, dim))

time: 448 us -> 654 us (1.46)
  waiting for transfers between devices: 189 us -> 369 us
  starting transfers between devices: 0.13 us -> 13.6 us
  blocking collectives: 90.2 us -> 97.1 us
    all_to_all x0 -> x1, waiting for transfers between devices: none -> 270 us  [exchange_gather(): parts = lax.all_to_all(parts, axis, split_axis=0, concat_axis=0)]
    all_gather x1 -> x0, waiting for transfers between devices: 89.1 us -> none  [turned_gather(): filled, at, done = (lax.all_gather(both, axis, axis=0, tiled=True), 0, [])]
    all_to_all x0 -> x1, starting transfers between devices: none -> 13.4 us  [exchange_gather(): parts = lax.all_to_all(parts, axis, split_axis=0, concat_axis=0)]
    all_gather x10, blocking collectives: 68.8 us -> 75.7 us  [carried_in(): pieces = jax.tree.map(lambda part: lax.all_gather(part, axis), total)]
    unnamed x78 -> x76, local copies, waits for them, and re-layouts: 33.2 us -> 32.5 us
  transfers between devices with their start and end apart: 4 -> 4, of which waited for: 3 -> 3; matrix products, arithmetic and copies ran while one was open for 6% -> 4% of each run, Pallas kernels for 0% -> 0%
where the time goes in v1:
time: 654 us; the launch traced here: 651 us
  waiting for transfers between devices  369 us (56%)
  local copies, waits for them, and re-layouts  100 us (15%)
  blocking collectives  97.1 us (15%)
  matrix products  47.3 us (7%)
  between operations  13.9 us (2%)
  starting transfers between devices  13.6 us (2%)
  other arithmetic  9.42 us (1%)
    all_to_all x1, waiting for transfers between devices, exchange_gather(): parts = lax.all_to_all(parts, axis, split_axis=0, concat_axis=0)  270 us
    all_gather x1, waiting for transfers between devices, side_by_side(): lax.all_gather(both, axis, axis=dim, tiled=True)  91.6 us
    all_gather x10, blocking collectives, carried_in(): pieces = jax.tree.map(lambda part: lax.all_gather(part, axis), total)  75.7 us
    unnamed x76, local copies, waits for them, and re-layouts  32.5 us
    another operation x1, local copies, waits for them, and re-layouts, on_device(): key_piece.reshape(piece_rows // span_rows, span_rows, attend_heads, ATT_QK)  22.6 us
    all_to_all x1, blocking collectives, sent_and_summed(): lax.all_to_all(in_blocks(value, dim, count), axis, 0, 0, tiled=True)  21.4 us
    dot_general x10, matrix products, add_scores(): jnp.einsum('qhd,khd->hqk', query_final, key_piece, preferred_element_type...  16 us
    dot_general x9, matrix products, project(): jnp.dot(source, weight, preferred_element_type=jnp.float32)  15.9 us
  transfers between devices with their start and end apart: 4, of which 3 were waited for; matrix products, arithmetic and copies ran while one was open for 4% of the time, Pallas kernels for 0%

profile of v1, /device:TPU:1, one launch (start us, length us, event | category | flops | bytes accessed | tf_op | source)
XLA Modules:
  0.0 651.0 jit_solution(11422251342663893181)
XLA Ops:
  6.5 0.8 constant_dynamic-update-slice_fusion.8
  10.2 0.8 constant_dynamic-update-slice_fusion.3
  11.0 0.8 constant_dynamic-update-slice_fusion.2
  13.2 6.1 stack.2
  19.3 13.4 %all-to-all-start = ((bf16[64,32,3072]{2,1,0:T(8,128)(2,1)}), bf16[64,32,3072]{2,1,0:T(8,128)(2,1)}, u32[]{:S(2)}, u32[]{:S(2)}) async-start(bf16[64,32,3072]{2,1,0:T(8,128)(2,1)} %stack.2), calls=%async_computation | async-start | bytes 25165824 | tf_op jit(solution)/shard_map/all_to_all | solution.py:23
  34.3 1.0 multiply_cosine_fusion
  35.3 269.5 %all-to-all-done = bf16[64,32,3072]{2,1,0:T(8,128)(2,1)} async-done(((bf16[64,32,3072]{2,1,0:T(8,128)(2,1)}), bf16[64,32,3072]{2,1,0:T(8,128)(2,1)}, u32[]{:S(2)}, u32[]{:S(2)}) %all-to-all-start) | async-done | bytes 12582944 | tf_op jit(solution)/shard_map/all_to_all | solution.py:23
  304.9 1.6 fusion.43
  306.5 1.7 fusion.35
  308.3 2.2 multiply_reduce_fusion.2
  310.5 1.6 fusion.40
  313.3 5.9 all_gather.62
  319.1 8.1 %all_gather.63 = f32[4,2,128]{2,1,0:T(2,128)S(1)} all-gather(f32[1,2,128]{2,1,0:T(2,128)S(1)} %get-tuple-element.137), channel_id=1, replica_groups=mesh['sp_0'=8,'sp_1'=4,'sp_2'=2,'tp'=4] {'sp_1'}, dimensions={0}, use_global_device_ids=true | all-gather | bytes 5120 | tf_op jit(solution)/shard_map/all_gather | solution.py:49
  327.8 3.8 all_gather.55
  333.0 2.0 all-gather.1
  335.8 9.9 %all_gather.67 = f32[4,2,128,128]{3,2,1,0:T(8,128)S(1)} all-gather(f32[1,2,128,128]{3,2,1,0:T(8,128)S(1)} %bitcast_add_fusion.4), channel_id=1, replica_groups=mesh['sp_0'=8,'sp_1'=4,'sp_2'=2,'tp'=4] {'sp_1'}, dimensions={0}, use_global_device_ids=true | all-gather | bytes 655360 | tf_op jit(solution)/shard_map/all_gather | solution.py:49
  345.7 0.9 multiply_add_fusion
  346.6 1.3 convolution_convert_fusion
  348.0 6.7 %all_gather.56 = f32[4,2,128]{2,1,0:T(2,128)S(1)} all-gather(f32[1,2,128]{2,1,0:T(2,128)S(1)} %get-tuple-element.132), channel_id=1, replica_groups=mesh['sp_0'=8,'sp_1'=4,'sp_2'=2,'tp'=4] {'sp_1'}, dimensions={0}, use_global_device_ids=true | all-gather | bytes 5120 | tf_op jit(solution)/shard_map/all_gather | solution.py:49
  354.7 5.8 all-gather
  361.2 10.3 %all_gather.60 = f32[4,2,128,128]{3,2,1,0:T(8,128)S(1)} all-gather(f32[1,2,128,128]{3,2,1,0:T(8,128)S(1)} %bitcast_add_fusion.10), channel_id=1, replica_groups=mesh['sp_0'=8,'sp_1'=4,'sp_2'=2,'tp'=4] {'sp_1'}, dimensions={0}, use_global_device_ids=true | all-gather | bytes 655360 | tf_op jit(solution)/shard_map/all_gather | solution.py:49
  371.6 0.9 multiply_add_fusion.1
  372.4 3.7 multiply_reduce_fusion
  376.8 1.4 fusion.26
  379.4 0.8 subtract_convert_fusion
  382.1 1.9 fusion.42
  384.0 1.4 rev.17
  385.4 12.8 %all_gather.64 = f32[8,2,128]{2,1,0:T(2,128)S(1)} all-gather(f32[1,2,128]{2,1,0:T(2,128)S(1)} %get-tuple-element.126), channel_id=1, replica_groups=mesh['sp_0'=8,'sp_1'=4,'sp_2'=2,'tp'=4] {'sp_0'}, dimensions={0}, use_global_device_ids=true | all-gather | bytes 9216 | tf_op jit(solution)/shard_map/all_gather | solution.py:49
  398.2 10.4 %all_gather.57 = f32[8,2,128]{2,1,0:T(2,128)S(1)} all-gather(f32[1,2,128]{2,1,0:T(2,128)S(1)} %get-tuple-element.121), channel_id=1, replica_groups=mesh['sp_0'=8,'sp_1'=4,'sp_2'=2,'tp'=4] {'sp_0'}, dimensions={0}, use_global_device_ids=true | all-gather | bytes 9216 | tf_op jit(solution)/shard_map/all_gather | solution.py:49
  408.7 0.8 pad_maximum_fusion.3
  410.4 2.4 fusion.76
  413.5 7.7 %all-gather.6.cloned.1.call-done = f32[8,2,128,128]{3,2,1,0:T(8,128)} async-done(((f32[1,2,128,128]{3,2,1,0:T(8,128)}), f32[8,2,128,128]{3,2,1,0:T(8,128)}) %all-gather.6.cloned.1.call-update) | async-done | bytes 1048592 | tf_op jit(solution)/shard_map/all_gather | solution.py:49
  421.3 2.3 fusion.89
  424.1 2.8 fusion.46
  426.9 91.6 %all-gather.10.cloned.1.call-done = bf16[10240,640]{1,0:T(8,128)(2,1)} async-done(((bf16[160,640]{1,0:T(8,128)(2,1)}), bf16[10240,640]{1,0:T(8,128)(2,1)}) %all-gather.10.cloned.1.call-update) | async-done | bytes 13107216 | tf_op jit(solution)/shard_map/all_gather | solution.py:65
  518.5 4.3 split.8
  522.8 8.3 %reshape_reshape.6 = bf16[10,1024,2,128]{3,2,1,0:T(2,128)(2,1)} reshape(bf16[10240,256]{1,0:T(8,128)(2,1)} %split.8) | data formatting | bytes 10485760 | tf_op jit(solution)/shard_map/reshape;reshape | solution.py:311
  531.1 6.9 %split.9 = bf16[10240,384]{1,0:T(8,128)(2,1)} slice(bf16[10240,640]{1,0:T(8,128)(2,1)} %all-gather.10.cloned.1.call-done), slice={[0:10240], [0:384]} | slice | bytes 15728640 | tf_op jit(solution)/shard_map/split | solution.py:65
  538.0 22.6 %reshape_reshape.7 = bf16[10,1024,2,192]{3,2,1,0:T(2,128)(2,1)} reshape(bf16[10240,384]{1,0:T(8,128)(2,1)} %split.9) | data formatting | bytes 15728640 | tf_op jit(solution)/shard_map/reshape;reshape | solution.py:310
  560.6 25.7 %copy.109 = bf16[10,1024,2,192]{1,3,2,0:T(8,128)(2,1)} copy(bf16[10,1024,2,192]{3,2,1,0:T(2,128)(2,1)} %reshape_reshape.7) | data formatting | bytes 15728640
  586.3 34.0 %while.13 = (s32[]{:T(128)}, f32[160,2,128]{2,0,1:T(8,128)S(1)}, f32[2,160]{1,0:T(2,128)S(1)}, bf16[10,1024,2,128]{3,2,1,0:T(2,128)(2,1)}, bf16[10,1024,2,192]{1...) while((s32[]{:T(128)}, f32[160,2,128]{2,0,1:T(8,128)S(1)}, ...), condition=%wide.region_12.13_spmd.clone, body=%wide.region_10.12_spmd.clone.sunk | while | flops 210780480 | bytes 4125808 | solution.py:313
  586.3 1.4 constant_dynamic-slice_fusion.2
  587.7 1.6 fusion.302
  589.7 1.4 constant_dynamic-slice_fusion.2
  591.1 1.6 fusion.302
  593.1 1.4 constant_dynamic-slice_fusion.2
  594.5 1.6 fusion.302
  596.5 1.4 constant_dynamic-slice_fusion.2
  597.9 1.6 fusion.302
  599.9 1.4 constant_dynamic-slice_fusion.2
  601.3 1.6 fusion.302
  603.3 1.4 constant_dynamic-slice_fusion.2
  604.7 1.6 fusion.302
  606.7 1.4 constant_dynamic-slice_fusion.2
  608.1 1.6 fusion.302
  610.1 1.4 constant_dynamic-slice_fusion.2
  611.5 1.6 fusion.302
  613.5 1.4 constant_dynamic-slice_fusion.2
  614.9 1.6 fusion.302
  616.9 1.4 constant_dynamic-slice_fusion.2
  618.3 1.6 fusion.302
  620.5 1.7 convolution_add_fusion
  622.3 21.4 %all_to_all.10 = f32[4,40,2048]{2,1,0:T(8,128)S(1)} all-to-all(f32[4,40,2048]{2,1,0:T(8,128)S(1)} %bitcast.437), channel_id=1, replica_groups=mesh['sp_0'=8,'sp_1'=4,'sp_2'=2,'tp'=4] {'tp'}, dimensions={0} | all-to-all | bytes 2621440 | tf_op jit(solution)/shard_map/all_to_all | solution.py:75
  643.7 0.8 reduce_sum.88
  (173 shorter events, 19.9 us)
Async XLA Ops:
  6.5 370.3 %copy-start = (bf16[768,384]{1,0:T(8,128)(2,1)S(1)}, bf16[768,384]{1,0:T(8,128)(2,1)}, u32[]{:S(2)}) copy-start(bf16[768,384]{1,0:T(8,128)(2,1)} %param.37) | copy-start | bytes 1769476
  19.3 13.5 %copy-start.6 = (bf16[160,2048]{1,0:T(8,128)(2,1)S(1)}, bf16[160,2048]{1,0:T(8,128)(2,1)}, u32[]{:S(2)}) copy-start(bf16[160,2048]{1,0:T(8,128)(2,1)} %param.23) | copy-start | bytes 1966084
  19.3 13.8 %copy-start.27 = (bf16[2048,64]{0,1:T(8,128)(2,1)S(1)}, bf16[2048,64]{0,1:T(8,128)(2,1)}, u32[]{:S(2)}) copy-start(bf16[2048,64]{0,1:T(8,128)(2,1)} %param.34) | copy-start | bytes 786436
  19.3 13.8 %copy-start.28 = (f32[2048]{0:T(1024)S(1)}, f32[2048]{0:T(1024)}, u32[]{:S(2)}) copy-start(f32[2048]{0:T(1024)} %param.24) | copy-start | bytes 24580
  19.3 285.6 %all-to-all-start = ((bf16[64,32,3072]{2,1,0:T(8,128)(2,1)}), bf16[64,32,3072]{2,1,0:T(8,128)(2,1)}, u32[]{:S(2)}, u32[]{:S(2)}) async-start(bf16[64,32,3072]{2,1,0:T(8,128)(2,1)} %stack.2), calls=%async_computation | async-start | bytes 25165824 | tf_op jit(solution)/shard_map/all_to_all | solution.py:23
  32.8 1.5 copy-start.17
  32.8 377.6 %all-gather.8.cloned.1.call-start = ((), (), s32[]{:S(2)}) async-start(), calls=%async_computation.3 | async-start | bytes 1179648 | tf_op jit(solution)/shard_map/all_gather | solution.py:49
  33.1 339.3 %copy-start.21 = (f32[160]{0:T(256)}, f32[160]{0:T(256)S(1)}, u32[]{:S(2)}) copy-start(f32[160]{0:T(256)S(1)} %add_rsqrt_fusion.6) | copy-start | bytes 1924
  332.4 14.2 %copy-start.16 = (f32[512]{0:T(512)S(1)}, f32[512]{0:T(512)}, u32[]{:S(2)}) copy-start(f32[512]{0:T(512)} %param.36) | copy-start | bytes 6148
  335.0 12.9 %copy-start.2 = (f32[4,128,128]{2,1,0:T(8,128)}, f32[4,128,128]{2,1,0:T(8,128)S(1)}, u32[]{:S(2)}) copy-start(f32[4,128,128]{2,1,0:T(8,128)S(1)} %all-gather.1) | copy-start | bytes 786436
  346.6 74.7 %all-gather.6.cloned.1.call-start = ((), (), s32[]{:S(2)}) async-start(), calls=%async_computation.2 | async-start | bytes 1179648 | tf_op jit(solution)/shard_map/all_gather | solution.py:49
  348.0 24.4 %copy-start.29 = (f32[2048]{0:T(1024)S(1)}, f32[2048]{0:T(1024)}, u32[]{:S(2)}) copy-start(f32[2048]{0:T(1024)} %param.24) | copy-start | bytes 24580
  372.4 4.4 copy-start.15
  376.1 142.4 %all-gather.10.cloned.1.call-start = ((), (), s32[]{:S(2)}) async-start(), calls=%async_computation.4 | async-start | bytes 13312000 | tf_op jit(solution)/shard_map/all_gather | solution.py:65
  376.8 2.1 copy-start.11
  376.8 2.3 copy-start.18
  378.2 0.9 copy-start.19
  378.5 0.9 copy-start.7
  378.5 0.9 copy-start.8
  379.3 1.4 copy-start.12
  379.4 2.7 copy-start.22
  379.4 2.7 copy-start.30
  382.1 26.5 %copy-start.9 = (bf16[160,2,32]{2,0,1:T(8,128)(2,1)S(1)}, bf16[160,2,32]{2,0,1:T(8,128)(2,1)}, u32[]{:S(2)}) copy-start(bf16[160,2,32]{2,0,1:T(8,128)(2,1)} %get-tuple-element.97) | copy-start | bytes 61444
  382.1 26.5 %copy-start.10 = (bf16[160,2,32]{2,0,1:T(8,128)(2,1)S(1)}, bf16[160,2,32]{2,0,1:T(8,128)(2,1)}, u32[]{:S(2)}) copy-start(bf16[160,2,32]{2,0,1:T(8,128)(2,1)} %get-tuple-element.98) | copy-start | bytes 61444
  382.1 26.5 %copy-start.13 = (bf16[160,2,128]{2,0,1:T(8,128)(2,1)S(1)}, bf16[160,2,128]{2,0,1:T(8,128)(2,1)}, u32[]{:S(2)}) copy-start(bf16[160,2,128]{2,0,1:T(8,128)(2,1)} %slice.707) | copy-start | bytes 245764
  384.0 25.4 %copy-start.3 = (f32[20,2,8,128]{3,2,1,0:T(8,128)}, f32[20,2,8,128]{3,2,1,0:T(8,128)S(1)}, u32[]{:S(2)}) copy-start(f32[20,2,8,128]{3,2,1,0:T(8,128)S(1)} %fusion.42) | copy-start | bytes 491524
  385.4 24.5 %copy-start.5 = (f32[160,2,128]{2,0,1:T(8,128)S(1)}, f32[160,2,128]{2,0,1:T(8,128)}, u32[]{:S(2)}) copy-start(f32[160,2,128]{2,0,1:T(8,128)} %rev.17) | copy-start | bytes 491524
  408.6 1.7 copy-start.25
  408.6 1.7 copy-start.26
  410.4 10.9 %copy-start.4 = (f32[20,2,8,128]{3,2,1,0:T(8,128)S(1)}, f32[20,2,8,128]{3,2,1,0:T(8,128)}, u32[]{:S(2)}) copy-start(f32[20,2,8,128]{3,2,1,0:T(8,128)} %copy-done.3) | copy-start | bytes 491524
  410.4 10.9 %copy-start.23 = (f32[2,128]{1,0:T(2,128)S(1)}, f32[2,128]{1,0:T(2,128)}, u32[]{:S(2)}) copy-start(f32[2,128]{1,0:T(2,128)} %get-tuple-element.91) | copy-start | bytes 3076
  410.4 10.9 %copy-start.24 = (f32[2,128]{1,0:T(2,128)S(1)}, f32[2,128]{1,0:T(2,128)}, u32[]{:S(2)}) copy-start(f32[2,128]{1,0:T(2,128)} %get-tuple-element.92) | copy-start | bytes 3076
  421.3 2.8 copy-start.31
  421.3 2.8 copy-start.32
  560.6 25.7 %copy-start.14 = (bf16[160,2,192]{2,0,1:T(8,128)(2,1)S(1)}, bf16[160,2,192]{2,0,1:T(8,128)(2,1)}, u32[]{:S(2)}) copy-start(bf16[160,2,192]{2,0,1:T(8,128)(2,1)} %pad_maximum_fusion.3) | copy-start | bytes 368644
  586.3 34.2 %copy-start.20 = (f32[256]{0:T(256)S(1)}, f32[256]{0:T(256)}, u32[]{:S(2)}) copy-start(f32[256]{0:T(256)} %param.41) | copy-start | bytes 3076
  622.3 22.2 %copy-start.1 = (bf16[768,384]{1,0:T(8,128)(2,1)S(1)}, bf16[768,384]{1,0:T(8,128)(2,1)}, u32[]{:S(2)}) copy-start(bf16[768,384]{1,0:T(8,128)(2,1)} %param.37) | copy-start | bytes 1769476
Sparse Core Ops, SparseCore 0:
  346.7 36.6 all-gather.7
  385.1 36.1 all-gather.5
  424.0 94.4 all-gather.9
